TPU v7x, 32 devices: a whole 2x2x4 slice. The times are simulated.
32 devices in a mesh: sp: 4 (over y, x), tp: 8 (over z, core).
Axes of the slice: x: 2, y: 2, z: 4, core: 2. Of those that a mesh axis runs over, the one named last changes fastest.
Arguments:
- mix_in: bfloat16 [4096, 2048], P('sp', 'tp'), may hold values from -8 to 8
- gate_in: bfloat16 [4096, 2048], P('sp', 'tp'), may hold values from -6 to 6
- conv_w: float32 [4, 2048], P(None, 'tp'), may hold values from -3 to 3
- conv_b: float32 [2048], P('tp'), may hold values from -3 to 3
- decay_param: float32 [2, 2048], P(None, 'tp')
- recur_gate: float32 [2, 32, 64, 64], P(None, 'tp'), may hold values from -0.75 to 0.75
- recur_bias: float32 [2, 2048], P(None, 'tp'), may hold values from -4 to 4
- input_gate: float32 [2, 32, 64, 64], P(None, 'tp'), may hold values from -0.75 to 0.75
- input_bias: float32 [2, 2048], P(None, 'tp'), may hold values from -4 to 4
- residual: bfloat16 [4096, 2048], P(('sp', 'tp')), may hold values from -6 to 6
- out_proj: bfloat16 [2048, 2048], replicated, may hold values from -0.125 to 0.125
- norm_gain: float32 [3, 2048], replicated, may hold values from 0.1 to 1.9
- routes: int32 [4096, 2], P('sp'), may hold values from 0 to 15, all different within a row; in each aligned block of 128 rows (0 to 127, 128 to 255, ...) at most 32 rows name the same one
- route_wt: float32 [4096, 2], P('sp'), may hold values from 0.1 to 1
- exp_gate: bfloat16 [16, 2048, 1024], P('sp', None, 'tp'), may hold values from -0.125 to 0.125
- exp_up: bfloat16 [16, 2048, 1024], P('sp', None, 'tp'), may hold values from -0.125 to 0.125
- exp_down: bfloat16 [16, 1024, 2048], P('sp', 'tp'), may hold values from -0.1875 to 0.1875
Outputs:
- final: bfloat16 [4096, 2048], P(('sp', 'tp'))
Inputs may be any that keep to these rules, and one draw needn't show every extreme that they name: `routes`: in each aligned block of 128 tokens (the rows of one device in the expert layer) no expert is named more than 32 times, and in some block some expert exactly 32 times; a token's 2 experts differ.
All inputs are finite; a program needn't handle non-finite values.
Results may differ from a plain program's by a relative error of at most 0.008.
Values may be sent and summed in bfloat16 or wider, within the bound.
A program may use at most 128 MiB of HBM per device.

v0:
```python
import jax
import jax.numpy as jnp
from jax import lax
from jax.sharding import PartitionSpec as P

EPSILON = 1e-06
HIGHEST_MODE = lax.Precision.HIGHEST


def extended(cells, sides, width):
    for axis, dim in sides:
        count = lax.axis_size(axis)
        ends = count - 1
        head = lax.slice_in_dim(cells, 0, width, axis=dim)
        tail = lax.slice_in_dim(cells, cells.shape[dim] - width, cells.shape[dim], axis=dim)
        cells = jnp.concatenate(
            [
                lax.ppermute(tail, axis, [(i, (i + 1) % count) for i in range(ends)]),
                cells,
                lax.ppermute(head, axis, [((i + 1) % count, i) for i in range(ends)]),
            ],
            axis=dim,
        )
    return cells


def carried_in(part, axis, combine, identity, reverse):
    count = lax.axis_size(axis)
    place = lax.axis_index(axis)
    ahead = count - 1 - place if reverse else place
    gathered = jax.tree.map(lambda a: lax.all_gather(a, axis), part)
    state = jax.tree.map(lambda a, e: jnp.zeros_like(a) + jnp.asarray(e, a.dtype), part, identity)

    def one(lap, state):
        source = count - 1 - lap if reverse else lap
        return combine(
            state, jax.tree.map(lambda a: lax.dynamic_index_in_dim(a, source, 0, False), gathered)
        )

    return lax.fori_loop(0, ahead, one, state)


def norm_rows(values, gain):
    floats = values.astype(jnp.float32)
    return floats * lax.rsqrt(jnp.mean(floats * floats, axis=-1, keepdims=True) + EPSILON) * gain


def pair_join(earlier, later_pair):
    return (earlier[0] * later_pair[0], later_pair[0] * earlier[1] + later_pair[1])


def slot_table(route_rows, experts, capacity):
    row_count, top_count = route_rows.shape
    flattened = route_rows.reshape(row_count * top_count)
    matches = (flattened[:, None] == jnp.arange(experts, dtype=jnp.int32)[None, :]).astype(
        jnp.int32
    )
    earlier_hits = jnp.cumsum(matches, axis=0) - matches
    position = jnp.sum(earlier_hits * matches, axis=1)
    return (flattened * capacity + position).reshape(row_count, top_count)


def weight_table(slots, route_weights, total_slots):
    matches = slots[..., None] == jnp.arange(total_slots, dtype=jnp.int32)
    return jnp.sum(jnp.where(matches, route_weights[..., None], 0.0), axis=-2)


def block_matrix(blocks):
    heads, head_dim, _ = blocks.shape
    identity = jnp.eye(heads, dtype=blocks.dtype)
    return jnp.einsum("hij,hg->higj", blocks, identity).reshape(heads * head_dim, heads * head_dim)


def coefficients(conv_out, recur_blocks, recur_bias, input_blocks, input_bias, decay_param):
    recur_pre = jnp.dot(conv_out, block_matrix(recur_blocks), precision=HIGHEST_MODE)
    input_pre = jnp.dot(conv_out, block_matrix(input_blocks), precision=HIGHEST_MODE)
    recur_act = jax.nn.sigmoid(recur_pre + recur_bias)
    input_act = jax.nn.sigmoid(input_pre + input_bias)
    log_decay = -8.0 * recur_act * jax.nn.softplus(-decay_param)
    return (jnp.exp(log_decay), jnp.sqrt(-jnp.expm1(2.0 * log_decay)) * (input_act * conv_out))


def on_device(
    mix_in,
    gate_in,
    conv_w,
    conv_b,
    decay_param,
    recur_gate,
    recur_bias,
    input_gate,
    input_bias,
    residual,
    out_proj,
    norm_gain,
    routes,
    route_wt,
    exp_gate,
    exp_up,
    exp_down,
):
    seq_len = mix_in.shape[0]
    padded = extended(mix_in, (("sp", 0),), 2).astype(jnp.float32)
    conv_out = conv_b + padded[0:seq_len] * conv_w[0]
    for tap in range(1, conv_w.shape[0]):
        conv_out = conv_out + padded[tap : tap + seq_len] * conv_w[tap]
    fwd_decay, fwd_drive = coefficients(
        conv_out, recur_gate[0], recur_bias[0], input_gate[0], input_bias[0], decay_param[0]
    )
    bwd_decay, bwd_drive = coefficients(
        conv_out, recur_gate[1], recur_bias[1], input_gate[1], input_bias[1], decay_param[1]
    )
    fwd_prod, fwd_state = lax.associative_scan(pair_join, (fwd_decay, fwd_drive), axis=0)
    bwd_prod, bwd_state = lax.associative_scan(
        pair_join, (jnp.flip(bwd_decay, 0), jnp.flip(bwd_drive, 0)), axis=0
    )
    identity = (jnp.ones_like(fwd_prod[-1]), jnp.zeros_like(fwd_state[-1]))
    fwd_enter = carried_in((fwd_prod[-1], fwd_state[-1]), "sp", pair_join, identity, False)[1]
    bwd_enter = carried_in((bwd_prod[-1], bwd_state[-1]), "sp", pair_join, identity, True)[1]
    state_sum = fwd_state + fwd_prod * fwd_enter + jnp.flip(bwd_state + bwd_prod * bwd_enter, 0)
    mixed = (state_sum * jax.nn.gelu(gate_in.astype(jnp.float32))).astype(jnp.bfloat16)
    tok_rows = lax.all_to_all(mixed, "tp", split_axis=0, concat_axis=1, tiled=True)
    proj = jnp.dot(tok_rows, out_proj, preferred_element_type=jnp.float32).astype(jnp.bfloat16)
    proj = lax.optimization_barrier(proj)
    stream = (residual.astype(jnp.float32) + norm_rows(proj, norm_gain[0])).astype(jnp.bfloat16)
    stream = lax.optimization_barrier(stream)
    normed = norm_rows(stream, norm_gain[1]).astype(jnp.bfloat16)
    sp_count = lax.axis_size("sp")
    row_count = residual.shape[0]
    width_model = residual.shape[1]
    top_count = routes.shape[1]
    local_experts = exp_gate.shape[0]
    experts = local_experts * sp_count
    capacity = 2 * row_count * top_count // experts
    total_slots = experts * capacity
    own_start = lax.axis_index("tp") * row_count
    own_routes = lax.dynamic_slice_in_dim(routes, own_start, row_count, 0)
    own_weights = lax.dynamic_slice_in_dim(route_wt, own_start, row_count, 0)
    own_slots = slot_table(own_routes, experts, capacity)
    selector = jnp.sum(
        (own_slots[:, :, None] == jnp.arange(total_slots, dtype=jnp.int32)).astype(jnp.bfloat16),
        axis=1,
    )
    outgoing = jnp.einsum("rs,rd->sd", selector, normed, preferred_element_type=jnp.float32).astype(
        jnp.bfloat16
    )
    arrived = lax.all_to_all(
        outgoing.reshape(experts, capacity, width_model),
        "sp",
        split_axis=0,
        concat_axis=1,
        tiled=True,
    )
    gate_full, up_full = (
        lax.all_gather(exp_gate, "tp", axis=2, tiled=True),
        lax.all_gather(exp_up, "tp", axis=2, tiled=True),
    )
    gate_act = jnp.einsum("emd,edf->emf", arrived, gate_full, preferred_element_type=jnp.float32)
    up_act = jnp.einsum("emd,edf->emf", arrived, up_full, preferred_element_type=jnp.float32)
    hidden = (jax.nn.silu(gate_act) * up_act).astype(jnp.bfloat16)
    summed = jnp.einsum(
        "emf,efd->emd",
        hidden,
        lax.all_gather(exp_down, "tp", axis=1, tiled=True),
        preferred_element_type=jnp.float32,
    )
    out_rows = summed.astype(jnp.bfloat16).reshape(local_experts, sp_count, capacity, width_model)
    returned = lax.all_to_all(out_rows, "sp", split_axis=1, concat_axis=0, tiled=True)
    values = returned.reshape(total_slots, width_model).astype(jnp.float32)
    own_table = weight_table(own_slots, own_weights, total_slots)
    mixture = jnp.dot(own_table, values, precision=HIGHEST_MODE).astype(jnp.bfloat16)
    mixture = lax.optimization_barrier(mixture)
    return (stream.astype(jnp.float32) + norm_rows(mixture, norm_gain[2])).astype(jnp.bfloat16)


def solution(mesh):
    return jax.shard_map(
        on_device,
        mesh=mesh,
        in_specs=(
            P("sp", "tp"),
            P("sp", "tp"),
            P(None, "tp"),
            P("tp"),
            P(None, "tp"),
            P(None, "tp", None, None),
            P(None, "tp"),
            P(None, "tp", None, None),
            P(None, "tp"),
            P(("sp", "tp"), None),
            P(),
            P(),
            P("sp", None),
            P("sp", None),
            P("sp", None, "tp"),
            P("sp", None, "tp"),
            P("sp", "tp", None),
        ),
        out_specs=P(("sp", "tp"), None),
        check_vma=False,
    )
```

profile of v0, /device:TPU:0, one launch (start us, length us, event | category | flops | bytes accessed | tf_op | source)
XLA Modules:
  0.0 535.8 jit_solution(3942051647278810106)
XLA Ops:
  8.8 4.9 collective-permute-start
  25.6 2.2 slice.705
  135.0 4.7 slice.809
  139.8 2.6 slice.811
  142.3 4.8 slice.807
  147.1 2.6 slice.814
  246.5 2.2 fusion.46
  248.9 10.2 %all-gather.1 = f32[4,1,256]{2,1,0:T(1,128)S(1)} all-gather(f32[1,1,256]{2,1,0:T(1,128)S(1)} %add_bitcast_fusion.3), channel_id=1, replica_groups=mesh['sp'=4,'tp'=8] {'sp'}, dimensions={0}, use_global_device_ids=true | all-gather | bytes 5120 | tf_op jit(solution)/shard_map/all_gather | solution.py:31
  261.8 2.2 pad_maximum_fusion.1
  264.2 4.7 pad.282
  269.6 7.1 %all-gather = f32[4,1,256]{2,1,0:T(1,128)S(1)} all-gather(f32[1,1,256]{2,1,0:T(1,128)S(1)} %add_bitcast_fusion.4), channel_id=1, replica_groups=mesh['sp'=4,'tp'=8] {'sp'}, dimensions={0}, use_global_device_ids=true | all-gather | bytes 5120 | tf_op jit(solution)/shard_map/all_gather | solution.py:31
  277.3 5.0 slice.883
  282.3 4.9 slice.805
  290.2 2.7 pad.303
  293.9 2.2 fusion.45
  299.1 8.1 %all-gather.3 = f32[4,1,256]{2,1,0:T(1,128)S(1)} all-gather(f32[1,1,256]{2,1,0:T(1,128)S(1)} %add_bitcast_fusion.1), channel_id=1, replica_groups=mesh['sp'=4,'tp'=8] {'sp'}, dimensions={0}, use_global_device_ids=true | all-gather | bytes 5120 | tf_op jit(solution)/shard_map/all_gather | solution.py:31
  307.2 4.6 pad.323
  313.6 4.7 pad.322
  319.0 7.1 %all-gather.2 = f32[4,1,256]{2,1,0:T(1,128)S(1)} all-gather(f32[1,1,256]{2,1,0:T(1,128)S(1)} %add_bitcast_fusion.2), channel_id=1, replica_groups=mesh['sp'=4,'tp'=8] {'sp'}, dimensions={0}, use_global_device_ids=true | all-gather | bytes 5120 | tf_op jit(solution)/shard_map/all_gather | solution.py:31
  326.3 3.0 multiply_add_fusion.2
  329.3 9.0 %rev.6 = f32[1024,256]{1,0:T(8,128)} reverse(f32[1024,256]{1,0:T(8,128)} %multiply_add_fusion.2), dimensions={0} | reverse | bytes 2097152 | tf_op jit(solution)/shard_map/jit(_flip)/rev | solution.py:120
  338.3 3.1 fusion.38
  343.4 5.1 all-to-all-start
  349.4 30.4 %all-to-all-done = bf16[8,128,256]{1,2,0:T(8,128)(2,1)S(1)} async-done(((bf16[8,128,256]{1,2,0:T(8,128)(2,1)}), bf16[8,128,256]{1,2,0:T(8,128)(2,1)S(1)}, u32[]{:S(2)}, u32[]{:S(2)}) %all-to-all-start) | async-done | bytes 524320 | tf_op jit(solution)/shard_map/all_to_all | solution.py:122
  379.8 5.0 convolution_convert_fusion.2
  386.4 29.0 %all_to_all.52 = bf16[16,32,2048]{2,1,0:T(8,128)(2,1)S(1)} all-to-all(bf16[16,32,2048]{2,1,0:T(8,128)(2,1)S(1)} %bitcast.116), channel_id=1, replica_groups=mesh['sp'=4,'tp'=8] {'sp'}, dimensions={0} | all-to-all | bytes 4194304 | tf_op jit(solution)/shard_map/all_to_all | solution.py:147
  415.6 9.6 %fusion.92 = f32[4,128,1024]{2,1,0:T(8,128)} fusion(bf16[4,128,2048]{2,1,0:T(8,128)(2,1)S(1)} %bitcast.113, bf16[4,2048,1024]{2,1,0:T(8,128)(2,1)} %all-gather.8.cloned.1.call-done), kind=kOutput, calls=%fused_computation.258 | convolution fusion | flops 2147483648 | bytes 20971520 | tf_op jit(solution)/shard_map/emd,edf->emf/dot_general | solution.py:158
  425.1 52.0 %all-gather.12.cloned.1.call-done = bf16[4,1024,2048]{2,1,0:T(8,128)(2,1)} async-done(((bf16[4,128,2048]{2,1,0:T(8,128)(2,1)}), bf16[4,1024,2048]{2,1,0:T(8,128)(2,1)}) %all-gather.12.cloned.1.call-update) | async-done | bytes 16777232 | tf_op jit(solution)/shard_map/all_gather | solution.py:164
  477.2 17.5 %convolution_convert_fusion.1 = bf16[4,128,2048]{2,1,0:T(8,128)(2,1)} fusion(bf16[4,1024,2048]{2,1,0:T(8,128)(2,1)} %all-gather.12.cloned.1.call-done, f32[4,128,1024]{2,1,0:T(8,128)} %fusion.92, bf16[4,128,2048]{2,1,0:T(8,128)(2,1)S(1)} %bitcast.114, bf16[4,2048,1024]{2,1,0:T(8,128)(2,1)} %all-gather.10.cloned.1.call-done), kind=kOutput, calls=%fused_computation.7 | convolution fusion | flops 4299161600 | bytes 39845888 | tf_op jit(solution)/shard_map/emf,efd->emd/dot_general | solution.py:161
  494.7 3.1 copy.38
  497.9 3.7 all-to-all-start.2
  502.3 24.7 %all-to-all-done.2 = bf16[4,4,32,2048]{3,2,0,1:T(8,128)(2,1)S(1)} async-done(((bf16[4,4,32,2048]{3,2,0,1:T(8,128)(2,1)}), bf16[4,4,32,2048]{3,2,0,1:T(8,128)(2,1)S(1)}, u32[]{:S(2)}, u32[]{:S(2)}) %all-to-all-start.2) | async-done | bytes 2097184 | tf_op jit(solution)/shard_map/all_to_all | solution.py:168
  (574 shorter events, 237.8 us)
Async XLA Ops:
  6.5 409.0 %all-gather.8.cloned.1.call-start = ((), (), s32[]{:S(2)}) async-start(), calls=%async_computation.3 | async-start | bytes 18874368 | tf_op jit(solution)/shard_map/all_gather | solution.py:155
  7.3 417.8 %all-gather.10.cloned.1.call-start = ((), (), s32[]{:S(2)}) async-start(), calls=%async_computation.4 | async-start | bytes 18874368 | tf_op jit(solution)/shard_map/all_gather | solution.py:156
  8.1 469.1 %all-gather.12.cloned.1.call-start = ((), (), s32[]{:S(2)}) async-start(), calls=%async_computation.5 | async-start | bytes 18874368 | tf_op jit(solution)/shard_map/all_gather | solution.py:164
  8.8 12.3 %collective-permute-start = (bf16[2,256]{1,0:T(2,128)(2,1)S(1)}, bf16[2,256]{1,0:T(2,128)(2,1)S(1)}, u32[]{:S(2)}, u32[]{:S(2)}) collective-permute-start(bf16[2,256]{1,0:T(2,128)(2,1)S(1)} %get-tuple-element.168), channel_id=1, source_target_pairs={{0,8},{8,16},{16,24},{1,9},{9,17},{17,25},{2,10},{10,18},{18,26},{... | collective-permute-start | bytes 3080 | tf_op jit(solution)/shard_map/ppermute | solution.py:18
  13.7 7.4 %collective-permute-start.1 = (bf16[2,256]{1,0:T(2,128)(2,1)S(1)}, bf16[2,256]{1,0:T(2,128)(2,1)S(1)}, u32[]{:S(2)}, u32[]{:S(2)}) collective-permute-start(bf16[2,256]{1,0:T(2,128)(2,1)S(1)} %get-tuple-element.167), channel_id=1, source_target_pairs={{8,0},{16,8},{24,16},{9,1},{17,9},{25,17},{10,2},{18,10},{26,18},{... | collective-permute-start | bytes 3080 | tf_op jit(solution)/shard_map/ppermute | solution.py:20
  25.5 99.7 %copy-start.7 = (f32[1024,256]{1,0:T(8,128)}, f32[1024,256]{1,0:T(8,128)S(1)}, u32[]{:S(2)}) copy-start(f32[1024,256]{1,0:T(8,128)S(1)} %fusion.16) | copy-start | bytes 3145732
  248.9 20.0 %copy-start.2 = (f32[1024,256]{1,0:T(8,128)}, f32[1024,256]{1,0:T(8,128)S(1)}, u32[]{:S(2)}) copy-start(f32[1024,256]{1,0:T(8,128)S(1)} %pad.262) | copy-start | bytes 3145732
  261.8 25.4 %copy-start.4 = (f32[1024,256]{1,0:T(8,128)}, f32[1024,256]{1,0:T(8,128)S(1)}, u32[]{:S(2)}) copy-start(f32[1024,256]{1,0:T(8,128)S(1)} %pad.283) | copy-start | bytes 3145732
  264.0 23.2 %copy-start.47 = (f32[2,256]{1,0:T(2,128)S(1)}, f32[2,256]{1,0:T(2,128)}, u32[]{:S(2)}) copy-start(f32[2,256]{1,0:T(2,128)} %slice.859) | copy-start | bytes 6148
  264.0 23.2 %copy-start.48 = (f32[2,256]{1,0:T(2,128)S(1)}, f32[2,256]{1,0:T(2,128)}, u32[]{:S(2)}) copy-start(f32[2,256]{1,0:T(2,128)} %slice.860) | copy-start | bytes 6148
  264.0 23.2 %copy-start.49 = (f32[2,256]{1,0:T(2,128)S(1)}, f32[2,256]{1,0:T(2,128)}, u32[]{:S(2)}) copy-start(f32[2,256]{1,0:T(2,128)} %slice.858) | copy-start | bytes 6148
  264.0 23.2 %copy-start.50 = (f32[2,256]{1,0:T(2,128)S(1)}, f32[2,256]{1,0:T(2,128)}, u32[]{:S(2)}) copy-start(f32[2,256]{1,0:T(2,128)} %slice.862) | copy-start | bytes 6148
  264.0 23.2 %copy-start.38 = (f32[4,256]{1,0:T(4,128)S(1)}, f32[4,256]{1,0:T(4,128)}, u32[]{:S(2)}) copy-start(f32[4,256]{1,0:T(4,128)} %get-tuple-element.238) | copy-start | bytes 12292
  264.1 23.2 %copy-start.39 = (f32[4,256]{1,0:T(4,128)S(1)}, f32[4,256]{1,0:T(4,128)}, u32[]{:S(2)}) copy-start(f32[4,256]{1,0:T(4,128)} %get-tuple-element.239) | copy-start | bytes 12292
  264.1 23.4 %copy-start.43 = (f32[3,256]{1,0:T(4,128)S(1)}, f32[3,256]{1,0:T(4,128)}, u32[]{:S(2)}) copy-start(f32[3,256]{1,0:T(4,128)} %slice.851) | copy-start | bytes 9220
  264.1 23.4 %copy-start.44 = (f32[3,256]{1,0:T(4,128)S(1)}, f32[3,256]{1,0:T(4,128)}, u32[]{:S(2)}) copy-start(f32[3,256]{1,0:T(4,128)} %slice.868) | copy-start | bytes 9220
  264.1 23.4 %copy-start.78 = (f32[1,256]{1,0:T(1,128)S(1)}, f32[1,256]{1,0:T(1,128)}, u32[]{:S(2)}) copy-start(f32[1,256]{1,0:T(1,128)} %slice.1017) | copy-start | bytes 3076
  264.1 23.4 %copy-start.77 = (f32[1,256]{1,0:T(1,128)S(1)}, f32[1,256]{1,0:T(1,128)}, u32[]{:S(2)}) copy-start(f32[1,256]{1,0:T(1,128)} %slice.985) | copy-start | bytes 3076
  264.1 23.5 %copy-start.34 = (f32[7,256]{1,0:T(8,128)S(1)}, f32[7,256]{1,0:T(8,128)}, u32[]{:S(2)}) copy-start(f32[7,256]{1,0:T(8,128)} %slice.845) | copy-start | bytes 21508
  264.1 23.5 %copy-start.35 = (f32[7,256]{1,0:T(8,128)S(1)}, f32[7,256]{1,0:T(8,128)}, u32[]{:S(2)}) copy-start(f32[7,256]{1,0:T(8,128)} %slice.870) | copy-start | bytes 21508
  264.1 23.5 %copy-start.76 = (f32[1,256]{1,0:T(1,128)S(1)}, f32[1,256]{1,0:T(1,128)}, u32[]{:S(2)}) copy-start(f32[1,256]{1,0:T(1,128)} %slice.1016) | copy-start | bytes 3076
  264.1 23.6 %copy-start.75 = (f32[1,256]{1,0:T(1,128)S(1)}, f32[1,256]{1,0:T(1,128)}, u32[]{:S(2)}) copy-start(f32[1,256]{1,0:T(1,128)} %slice.984) | copy-start | bytes 3076
  264.1 23.6 %copy-start.30 = (f32[15,256]{1,0:T(8,128)S(1)}, f32[15,256]{1,0:T(8,128)}, u32[]{:S(2)}) copy-start(f32[15,256]{1,0:T(8,128)} %slice.839) | copy-start | bytes 46084
  264.2 23.6 %copy-start.31 = (f32[15,256]{1,0:T(8,128)S(1)}, f32[15,256]{1,0:T(8,128)}, u32[]{:S(2)}) copy-start(f32[15,256]{1,0:T(8,128)} %slice.872) | copy-start | bytes 46084
  264.2 23.7 %copy-start.74 = (f32[1,256]{1,0:T(1,128)S(1)}, f32[1,256]{1,0:T(1,128)}, u32[]{:S(2)}) copy-start(f32[1,256]{1,0:T(1,128)} %slice.1015) | copy-start | bytes 3076
  264.2 23.7 %copy-start.73 = (f32[1,256]{1,0:T(1,128)S(1)}, f32[1,256]{1,0:T(1,128)}, u32[]{:S(2)}) copy-start(f32[1,256]{1,0:T(1,128)} %slice.983) | copy-start | bytes 3076
  264.2 23.8 %copy-start.26 = (f32[31,256]{1,0:T(8,128)S(1)}, f32[31,256]{1,0:T(8,128)}, u32[]{:S(2)}) copy-start(f32[31,256]{1,0:T(8,128)} %slice.833) | copy-start | bytes 95236
  264.2 23.8 %copy-start.27 = (f32[31,256]{1,0:T(8,128)S(1)}, f32[31,256]{1,0:T(8,128)}, u32[]{:S(2)}) copy-start(f32[31,256]{1,0:T(8,128)} %slice.874) | copy-start | bytes 95236
  268.9 19.1 %copy-start.64 = (f32[1,256]{1,0:T(1,128)S(1)}, f32[1,256]{1,0:T(1,128)}, u32[]{:S(2)}) copy-start(f32[1,256]{1,0:T(1,128)} %slice.1014) | copy-start | bytes 3076
  268.9 19.2 %copy-start.63 = (f32[1,256]{1,0:T(1,128)S(1)}, f32[1,256]{1,0:T(1,128)}, u32[]{:S(2)}) copy-start(f32[1,256]{1,0:T(1,128)} %slice.982) | copy-start | bytes 3076
  343.4 36.4 %all-to-all-start = ((bf16[8,128,256]{1,2,0:T(8,128)(2,1)}), bf16[8,128,256]{1,2,0:T(8,128)(2,1)S(1)}, u32[]{:S(2)}, u32[]{:S(2)}) async-start(bf16[8,128,256]{1,2,0:T(8,128)(2,1)} %copy.33), calls=%async_computation | async-start | bytes 1048576 | tf_op jit(solution)/shard_map/all_to_all | solution.py:122
  497.9 29.1 %all-to-all-start.2 = ((bf16[4,4,32,2048]{3,2,0,1:T(8,128)(2,1)}), bf16[4,4,32,2048]{3,2,0,1:T(8,128)(2,1)S(1)}, u32[]{:S(2)}, u32[]{:S(2)}) async-start(bf16[4,4,32,2048]{3,2,0,1:T(8,128)(2,1)} %copy.38), calls=%async_computation.2 | async-start | bytes 4194304 | tf_op jit(solution)/shard_map/all_to_all | solution.py:168
  (69 other events, 455.8 us)
Sparse Core Ops, SparseCore 0:
  8.9 154.5 all-gather.7
  165.1 149.9 all-gather.9
  316.7 160.4 all-gather.11
where the time goes:
time: 543 us; the launch traced here: 536 us
  local copies, waits for them, and re-layouts  243 us (45%)
  waiting for transfers between devices  109 us (20%)
  blocking collectives  61.5 us (11%)
  other arithmetic  50.5 us (9%)
  matrix products  40.5 us (7%)
  between operations  15.5 us (3%)
  starting transfers between devices  15 us (3%)
    slice x74, local copies, waits for them, and re-layouts, on_device(): lax.associative_scan(pair_join, (jnp.flip(bwd_decay, 0), jnp.flip(bwd_dri...  109 us
    slice x69, local copies, waits for them, and re-layouts, on_device(): lax.associative_scan(pair_join, (fwd_decay, fwd_drive), axis=0)  87.7 us
    all_gather x1, waiting for transfers between devices, on_device(): lax.all_gather(exp_down, 'tp', axis=1, tiled=True)  52 us
    all_gather x4, blocking collectives, carried_in(): gathered = jax.tree.map(lambda a: lax.all_gather(a, axis), part)  32.5 us
    all_to_all x1, waiting for transfers between devices, on_device(): lax.all_to_all(mixed, 'tp', split_axis=0, concat_axis=1, tiled=True)  30.4 us
    add x37, other arithmetic, pair_join(): later_pair[0] * earlier[1] + later_pair[1]  30 us
    all_to_all x1, blocking collectives, on_device(): lax.all_to_all(outgoing.reshape(experts, capacity, width_model), 'sp', sp...  29 us
    all_to_all x1, waiting for transfers between devices, on_device(): lax.all_to_all(out_rows, 'sp', split_axis=1, concat_axis=0, tiled=True)  24.7 us
  transfers between devices with their start and end apart: 7, of which 3 were waited for; matrix products, arithmetic and copies ran while one was open for 58% of the time, Pallas kernels for 0%

commit v1 on v0

v1 whole, which is shorter than its diff:
```python
import functools

import jax
import jax.numpy as jnp
from jax import lax
from jax.experimental import pallas as pl
from jax.experimental.pallas import tpu as pltpu
from jax.sharding import PartitionSpec as P

EPSILON = 1e-06
HIGHEST_MODE = lax.Precision.HIGHEST
MESH = pl.DeviceIdType.MESH
HALO = 16
SUB = 8


def norm_rows(values, gain):
    floats = values.astype(jnp.float32)
    return floats * lax.rsqrt(jnp.mean(floats * floats, axis=-1, keepdims=True) + EPSILON) * gain


def slot_table(route_rows, experts, capacity):
    row_count, top_count = route_rows.shape
    flattened = route_rows.reshape(row_count * top_count)
    matches = flattened[:, None] == jnp.arange(experts, dtype=jnp.int32)[None, :]
    order = jnp.arange(row_count * top_count, dtype=jnp.int32)
    before = (order[None, :] < order[:, None]).astype(jnp.bfloat16)
    earlier_hits = jnp.dot(
        before, matches.astype(jnp.bfloat16), preferred_element_type=jnp.float32
    )
    position = jnp.sum(jnp.where(matches, earlier_hits, 0.0), axis=1).astype(jnp.int32)
    return (flattened * capacity + position).reshape(row_count, top_count)


def weight_table(slots, route_weights, total_slots):
    matches = slots[..., None] == jnp.arange(total_slots, dtype=jnp.int32)
    return jnp.sum(jnp.where(matches, route_weights[..., None], 0.0), axis=-2)


def one_minus_exp(y):
    series = -y * (1.0 + y * (1.0 / 2) * (1.0 + y * (1.0 / 3) * (1.0 + y * 0.25 * (1.0 + y * 0.2))))
    return jnp.where(y > -0.1, series, 1.0 - jnp.exp(y))


def split_f32(x):
    high = x.astype(jnp.bfloat16)
    return high, (x - high.astype(jnp.float32)).astype(jnp.bfloat16)


def tile_scan(a, b, reverse):
    row = lax.broadcasted_iota(jnp.int32, a.shape, 1)
    step = 1
    while step < SUB:
        shift = SUB - step if reverse else step
        keep = row < SUB - step if reverse else row >= step
        a_prev = jnp.where(keep, pltpu.roll(a, shift, 1), 1.0)
        b_prev = jnp.where(keep, pltpu.roll(b, shift, 1), 0.0)
        b = b + a * b_prev
        a = a * a_prev
        step *= 2
    return a, b


def mixer_kernel(
    dims,
    mix_ref, gate_ref, cw_ref, cb_ref, soft_ref, rg_ref, rb_ref, ig_ref, ib_ref,
    res_ref, gain_ref, slots_ref, op_hbm, eg_hbm, eu_hbm, ed_hbm,
    stream_ref, arrived_hbm, gf_hbm, uf_hbm, df_hbm,
    xp, wh, wl, af, bf, ab, bb, mixed, tok, op, proj, outgoing, halo, summ, ends,
    bg, bu, bd,
    op_sem, own_sem, halo_send, halo_recv, sum_send, sum_recv,
    mix_send, mix_recv, dis_send, dis_recv, z_send, z_recv, c_send, c_recv,
):
    S, T, L, G = dims
    seq, C = mix_ref.shape
    rows, D = res_ref.shape
    slots = outgoing.shape[0]
    cap = slots // (S * L)
    heads, hd = rg_ref.shape[1], rg_ref.shape[2]
    F = eg_hbm.shape[2]
    sp = lax.axis_index("sp")
    tp = lax.axis_index("tp")
    q = tp // G
    g = lax.rem(tp, G)

    def place_of(dq, dg):
        return lax.rem(q + dq, L) * G + lax.rem(g + dg, G)

    op_copy = pltpu.make_async_copy(op_hbm, op, op_sem)
    op_copy.start()
    own_in = [
        pltpu.make_async_copy(h.at[q], v, own_sem.at[i])
        for i, (h, v) in enumerate(((eg_hbm, bg), (eu_hbm, bu), (ed_hbm, bd)))
    ]
    for c in own_in:
        c.start()

    barrier = pltpu.get_barrier_semaphore()
    greeted = 0
    for ds in range(S):
        for dq in range(L):
            for dg in range(G):
                if (ds or dq or dg) and (ds == 0 or dg == 0):
                    pl.semaphore_signal(
                        barrier, inc=1,
                        device_id=(lax.rem(sp + ds, S), place_of(dq, dg)),
                        device_id_type=MESH,
                    )
                    greeted += 1
    pl.semaphore_wait(barrier, greeted)

    def remote(src, dst, send, recv, sp_to, tp_to):
        return pltpu.make_async_remote_copy(
            src_ref=src, dst_ref=dst, send_sem=send, recv_sem=recv,
            device_id=(sp_to, tp_to), device_id_type=MESH,
        )

    to_next = remote(mix_ref.at[pl.ds(seq - HALO, HALO)], halo.at[0], halo_send.at[0],
                     halo_recv.at[0], lax.rem(sp + 1, S), tp)
    to_prev = remote(mix_ref.at[pl.ds(0, HALO)], halo.at[1], halo_send.at[1],
                     halo_recv.at[1], lax.rem(sp + S - 1, S), tp)
    to_next.start()
    to_prev.start()

    def full_slot(ref, axis, place):
        if len(ref.shape) == 3:
            return ref.at[place]
        start = pl.multiple_of(place * F, F)
        return ref.at[:, pl.ds(start, F)] if axis else ref.at[pl.ds(start, F), :]

    tensors = ((eg_hbm, gf_hbm, 1), (eu_hbm, uf_hbm, 1), (ed_hbm, df_hbm, 0))

    def z_copies(dq):
        return [
            remote(src.at[lax.rem(q + dq, L)], full_slot(dst, axis, tp), z_send.at[dq, i],
                   z_recv.at[dq, i], sp, place_of(dq, 0))
            for i, (src, dst, axis) in enumerate(tensors)
        ]

    def core_copies(dq, i, own):
        src, dst, axis = tensors[i]
        origin = place_of(L - dq, 0)
        at = full_slot(dst, axis, origin)
        return [
            remote(own if own is not None else at, at, c_send.at[dq, dg, i], c_recv.at[dq, dg, i],
                   sp, place_of(0, dg))
            for dg in range(1, G)
        ]

    far = [dq for dq in range(1, L) if min(dq, L - dq) > 1]
    near = [dq for dq in range(1, L) if min(dq, L - dq) == 1]
    z_all = {dq: z_copies(dq) for dq in range(1, L)}
    for i in range(3):
        for dq in near:
            z_all[dq][i].start()
    own_out, core_all = [], {}
    for i, (src, dst, axis) in enumerate(tensors):
        core_all[0, i] = core_copies(0, i, src.at[q])
        for c in core_all[0, i]:
            c.start()
    for i, (buf, (src, dst, axis)) in enumerate(zip((bg, bu, bd), tensors)):
        own_in[i].wait()
        c = pltpu.make_async_copy(buf, full_slot(dst, axis, tp), own_sem.at[3 + i])
        c.start()
        own_out.append(c)

    wh[...] = jnp.zeros_like(wh)
    wl[...] = jnp.zeros_like(wl)
    for k, ref in enumerate((rg_ref, ig_ref)):
        for sense in range(2):
            for h in range(heads):
                high, low = split_f32(ref[sense, h])
                col = (2 * sense + k) * C + h * hd
                wh[h * hd : (h + 1) * hd, col : col + hd] = high
                wl[h * hd : (h + 1) * hd, col : col + hd] = low
    xp[SUB : SUB + seq, :] = mix_ref[...].astype(jnp.float32)
    to_next.wait()
    to_prev.wait()
    tail = halo[0].astype(jnp.float32)[HALO - SUB : HALO]
    head = halo[1].astype(jnp.float32)[0:SUB]
    xp[0:SUB, :] = jnp.where(sp > 0, tail, 0.0)
    xp[SUB + seq : 2 * SUB + seq, :] = jnp.where(sp < S - 1, head, 0.0)

    R = min(128, seq)

    def gates(n, _):
        base = pl.multiple_of(n * R, R)
        window = xp[pl.ds(base, R + 2 * SUB), :]
        conv = cb_ref[...] + window[SUB - 2 : SUB - 2 + R] * cw_ref[0:1]
        for tap in range(1, cw_ref.shape[0]):
            conv = conv + window[SUB - 2 + tap : SUB - 2 + tap + R] * cw_ref[tap : tap + 1]
        high, low = split_f32(conv)
        for sense, (a_ref, b_ref) in enumerate(((af, bf), (ab, bb))):
            cols = slice(2 * sense * C, (2 * sense + 2) * C)
            pre = jnp.dot(high, wh[:, cols], preferred_element_type=jnp.float32)
            pre = pre + jnp.dot(low, wh[:, cols], preferred_element_type=jnp.float32)
            pre = pre + jnp.dot(high, wl[:, cols], preferred_element_type=jnp.float32)
            recur = jax.nn.sigmoid(pre[:, :C] + rb_ref[sense : sense + 1])
            inp = jax.nn.sigmoid(pre[:, C:] + ib_ref[sense : sense + 1])
            log_a = -8.0 * recur * soft_ref[sense : sense + 1]
            a = jnp.exp(log_a)
            b = jnp.sqrt(one_minus_exp(2.0 * log_a)) * (inp * conv)
            a, b = tile_scan(
                a.reshape(R // SUB, SUB, C), b.reshape(R // SUB, SUB, C), sense == 1
            )
            a_ref[pl.ds(base, R), :] = a.reshape(R, C)
            b_ref[pl.ds(base, R), :] = b.reshape(R, C)
        return 0

    lax.fori_loop(0, seq // R, gates, 0)

    tiles = seq // SUB

    def carry(t, held):
        sf, pf, sb, pb = held
        at = pl.ds(pl.multiple_of(t * SUB, SUB), SUB)
        a = af[at, :]
        s = bf[at, :] + a * sf
        p = a * pf
        af[at, :] = p
        bf[at, :] = s
        back = pl.ds(pl.multiple_of((tiles - 1 - t) * SUB, SUB), SUB)
        a = ab[back, :]
        s2 = bb[back, :] + a * sb
        p2 = a * pb
        ab[back, :] = p2
        bb[back, :] = s2
        return s[SUB - 1 : SUB], p[SUB - 1 : SUB], s2[0:1], p2[0:1]

    zero, one = jnp.zeros((1, C), jnp.float32), jnp.ones((1, C), jnp.float32)
    sf, pf, sb, pb = lax.fori_loop(0, tiles, carry, (zero, one, zero, one), unroll=4)
    summ[0:1, :] = sf
    summ[1:2, :] = pf
    summ[2:3, :] = sb
    summ[3:4, :] = pb
    sums = [
        remote(summ, ends.at[ds - 1], sum_send.at[ds - 1], sum_recv.at[ds - 1],
               lax.rem(sp + ds, S), tp)
        for ds in range(1, S)
    ]
    for c in sums:
        c.start()
    for c in sums:
        c.wait()
    fe, be = zero, zero
    for ds in range(S - 1, 0, -1):
        fe = jnp.where(sp >= ds, ends[ds - 1, 1:2, :] * fe + ends[ds - 1, 0:1, :], fe)
    for ds in range(1, S):
        be = jnp.where(sp + S - ds < S, ends[ds - 1, 3:4, :] * be + ends[ds - 1, 2:3, :], be)

    def join(n, _):
        at = pl.ds(pl.multiple_of(n * R, R), R)
        state = (bf[at, :] + af[at, :] * fe) + (bb[at, :] + ab[at, :] * be)
        mixed[at, :] = (state * jax.nn.gelu(gate_ref[at, :].astype(jnp.float32))).astype(
            jnp.bfloat16
        )
        return 0

    lax.fori_loop(0, seq // R, join, 0)

    def block_rows(place):
        return mixed.at[pl.ds(pl.multiple_of(place * rows, rows), rows), :]

    columns = pl.ds(pl.multiple_of(tp * C, C), C)
    moves = []
    for dq in range(L):
        for dg in range(G):
            if dq or dg:
                k = dq * G + dg
                to = place_of(dq, dg)
                moves.append(remote(block_rows(to), tok.at[:, columns], mix_send.at[k],
                                    mix_recv.at[k], sp, to))
    for c in moves:
        c.start()
    own_move = pltpu.make_async_copy(block_rows(tp), tok.at[:, columns], own_sem.at[6])
    own_move.start()
    for dq in far:
        for c in z_all[dq]:
            c.start()
    op_copy.wait()
    own_move.wait()
    for c in moves:
        c.wait()

    def project(n, _):
        cols = pl.ds(pl.multiple_of(n * 256, 256), 256)
        proj[:, cols] = (
            jnp.dot(tok[...], op[:, cols], preferred_element_type=jnp.float32)
            .astype(jnp.bfloat16)
        )
        return 0

    lax.fori_loop(0, D // 256, project, 0)
    part = 32

    def norms(n, _):
        at = pl.ds(pl.multiple_of(n * part, part), part)
        s = (
            res_ref[at, :].astype(jnp.float32) + norm_rows(proj[at, :], gain_ref[0:1, :])
        ).astype(jnp.bfloat16)
        stream_ref[at, :] = s
        tok[at, :] = norm_rows(s, gain_ref[1:2, :]).astype(jnp.bfloat16)
        return 0

    lax.fori_loop(0, rows // part, norms, 0)
    slot_id = lax.broadcasted_iota(jnp.int32, (slots, rows), 0)
    hit = slot_id == slots_ref[0:1, :]
    for k in range(1, slots_ref.shape[0]):
        hit = hit | (slot_id == slots_ref[k : k + 1, :])
    selector = jnp.where(hit, 1.0, 0.0).astype(jnp.bfloat16)

    def dispatch(n, _):
        cols = pl.ds(pl.multiple_of(n * 256, 256), 256)
        outgoing[:, cols] = (
            jnp.dot(selector, tok[:, cols], preferred_element_type=jnp.float32)
            .astype(jnp.bfloat16)
        )
        return 0

    lax.fori_loop(0, D // 256, dispatch, 0)
    sends = []
    mine = sp * L + q
    for ds in range(S):
        for dq in range(L):
            sp_to, q_to = lax.rem(sp + ds, S), lax.rem(q + dq, L)
            src = outgoing.at[pl.ds(pl.multiple_of((sp_to * L + q_to) * cap, cap), cap), :]
            if ds or dq:
                k = ds * L + dq
                sends.append(remote(src, arrived_hbm.at[mine], dis_send.at[k], dis_recv.at[k],
                                    sp_to, q_to * G + g))
            else:
                sends.append(pltpu.make_async_copy(src, arrived_hbm.at[mine], own_sem.at[7]))
    for c in sends:
        c.start()
    for dq in near + far:
        for i in range(3):
            z_all[dq][i].wait_recv()
            core_all[dq, i] = core_copies(dq, i, None)
            for c in core_all[dq, i]:
                c.start()
    for c in sends:
        c.wait()
    for dq in range(1, L):
        for c in z_all[dq]:
            c.wait_send()
    for c in own_out:
        c.wait()
    for group in core_all.values():
        for c in group:
            c.wait()


def return_kernel(dims, rows_hbm, back_hbm, own_sem, send, recv):
    S, T, L, G = dims
    sp = lax.axis_index("sp")
    tp = lax.axis_index("tp")
    q = tp // G
    g = lax.rem(tp, G)
    barrier = pltpu.get_barrier_semaphore()
    peers = [
        (ds, dq, lax.rem(sp + ds, S), lax.rem(q + dq, L))
        for ds in range(S) for dq in range(L) if ds or dq
    ]
    for ds, dq, sp_to, q_to in peers:
        pl.semaphore_signal(
            barrier, inc=1, device_id=(sp_to, q_to * G + g), device_id_type=MESH
        )
    pl.semaphore_wait(barrier, len(peers))
    mine = sp * L + q
    copies = [
        pltpu.make_async_remote_copy(
            src_ref=rows_hbm.at[sp_to * L + q_to], dst_ref=back_hbm.at[mine],
            send_sem=send.at[ds * L + dq], recv_sem=recv.at[ds * L + dq],
            device_id=(sp_to, q_to * G + g), device_id_type=MESH,
        )
        for ds, dq, sp_to, q_to in peers
    ]
    copies.append(pltpu.make_async_copy(rows_hbm.at[mine], back_hbm.at[mine], own_sem))
    for c in copies:
        c.start()
    for c in copies:
        c.wait()


def on_device(
    mix_in, gate_in, conv_w, conv_b, decay_param, recur_gate, recur_bias, input_gate, input_bias,
    residual, out_proj, norm_gain, routes, route_wt, exp_gate, exp_up, exp_down,
):
    S, T = lax.axis_size("sp"), lax.axis_size("tp")
    L, D, F = exp_gate.shape
    G = T // L
    dims = (S, T, L, G)
    seq, C = mix_in.shape
    rows = residual.shape[0]
    top_count = routes.shape[1]
    experts = L * S
    cap = 2 * rows * top_count // experts
    total_slots = experts * cap
    own_start = lax.axis_index("tp") * rows
    own_routes = lax.dynamic_slice_in_dim(routes, own_start, rows, 0)
    own_weights = lax.dynamic_slice_in_dim(route_wt, own_start, rows, 0)
    own_slots = slot_table(own_routes, experts, cap)
    soft = jax.nn.softplus(-decay_param)
    wide = F % 128 == 0
    vmem = pl.BlockSpec(memory_space=pltpu.VMEM)
    hbm = pl.BlockSpec(memory_space=pltpu.MemorySpace.HBM)
    b16, f32 = jnp.bfloat16, jnp.float32
    dma = pltpu.SemaphoreType.DMA
    sds = jax.ShapeDtypeStruct
    up_shape = (D, T * F) if wide else (T, D, F)
    down_shape = (T * F, D) if wide else (T, F, D)
    stream, arrived, gate_full, up_full, down_full = pl.pallas_call(
        functools.partial(mixer_kernel, dims),
        out_shape=(
            sds((rows, D), b16), sds((experts, cap, D), b16),
            sds(up_shape, b16), sds(up_shape, b16), sds(down_shape, b16),
        ),
        in_specs=[vmem] * 12 + [hbm] * 4,
        out_specs=(vmem, hbm, hbm, hbm, hbm),
        scratch_shapes=[
            pltpu.VMEM((seq + 2 * SUB, C), f32),
            pltpu.VMEM((C, 4 * C), b16),
            pltpu.VMEM((C, 4 * C), b16),
            pltpu.VMEM((seq, C), f32), pltpu.VMEM((seq, C), f32),
            pltpu.VMEM((seq, C), f32), pltpu.VMEM((seq, C), f32),
            pltpu.VMEM((seq, C), b16),
            pltpu.VMEM((rows, T * C), b16),
            pltpu.VMEM(out_proj.shape, b16),
            pltpu.VMEM((rows, D), b16),
            pltpu.VMEM((total_slots, D), b16),
            pltpu.VMEM((2, HALO, C), b16),
            pltpu.VMEM((SUB, C), f32),
            pltpu.VMEM((S - 1, SUB, C), f32),
            pltpu.VMEM((D, F), b16), pltpu.VMEM((D, F), b16), pltpu.VMEM((F, D), b16),
            dma, dma((8,)),
            dma((2,)), dma((2,)),
            dma((S - 1,)), dma((S - 1,)),
            dma((T,)), dma((T,)),
            dma((experts,)), dma((experts,)),
            dma((L, 3)), dma((L, 3)),
            dma((L, G, 3)), dma((L, G, 3)),
        ],
        compiler_params=pltpu.CompilerParams(
            collective_id=0, has_side_effects=True, vmem_limit_bytes=56 * 1024 * 1024
        ),
    )(
        mix_in, gate_in, conv_w, conv_b.reshape(1, C), soft, recur_gate, recur_bias, input_gate,
        input_bias, residual, norm_gain, own_slots.T, out_proj, exp_gate, exp_up, exp_down,
    )
    flat = arrived.reshape(total_slots, D)
    if wide:
        gate_act = jnp.dot(flat, gate_full, preferred_element_type=f32)
        up_act = jnp.dot(flat, up_full, preferred_element_type=f32)
    else:
        gate_act = jnp.einsum("md,tdf->mtf", flat, gate_full, preferred_element_type=f32)
        up_act = jnp.einsum("md,tdf->mtf", flat, up_full, preferred_element_type=f32)
    hidden = (jax.nn.silu(gate_act) * up_act).astype(b16).reshape(total_slots, T * F)
    out_rows = jnp.dot(
        hidden, down_full.reshape(T * F, D), preferred_element_type=f32
    ).astype(b16)
    returned = pl.pallas_call(
        functools.partial(return_kernel, dims),
        out_shape=sds((experts, cap, D), b16),
        in_specs=[hbm],
        out_specs=hbm,
        scratch_shapes=[dma, dma((experts,)), dma((experts,))],
        compiler_params=pltpu.CompilerParams(collective_id=1, has_side_effects=True),
    )(out_rows.reshape(experts, cap, D))
    values = returned.reshape(total_slots, D).astype(f32)
    own_table = weight_table(own_slots, own_weights, total_slots)
    mixture = jnp.dot(own_table, values, precision=HIGHEST_MODE).astype(b16)
    mixture = lax.optimization_barrier(mixture)
    return (stream.astype(f32) + norm_rows(mixture, norm_gain[2])).astype(b16)


def solution(mesh):
    return jax.shard_map(
        on_device,
        mesh=mesh,
        in_specs=(
            P("sp", "tp"),
            P("sp", "tp"),
            P(None, "tp"),
            P("tp"),
            P(None, "tp"),
            P(None, "tp", None, None),
            P(None, "tp"),
            P(None, "tp", None, None),
            P(None, "tp"),
            P(("sp", "tp"), None),
            P(),
            P(),
            P("sp", None),
            P("sp", None),
            P("sp", None, "tp"),
            P("sp", None, "tp"),
            P("sp", "tp", None),
        ),
        out_specs=P(("sp", "tp"), None),
        check_vma=False,
    )
```

time: 543 us -> 277 us (0.51); the launches traced: 536 us -> 277 us
  Pallas kernels: 0 us -> 251 us
  local copies, waits for them, and re-layouts: 243 us -> 1.94 us
  waiting for transfers between devices: 109 us -> 0 us
  blocking collectives: 61.5 us -> 0 us
  other arithmetic: 50.5 us -> 3.92 us
  matrix products: 40.5 us -> 19.5 us
  between operations: 15.5 us -> 0.11 us
  starting transfers between devices: 15 us -> 0 us
    pallas_call x0 -> x2, Pallas kernels: none -> 251 us  [the longest x1 200 us: on_device(): pl.pallas_call(functools.partial(mixer_kernel, dims), out_shape=(sds((row...]
    slice x149 -> x1, local copies, waits for them, and re-layouts: 198 us -> 0.78 us  [on_device(): return (stream.astype(f32) + norm_rows(mixture, norm_gain[2])).astype(b16)]
    all_to_all x2 -> x0, waiting for transfers between devices: 55.1 us -> none  [the longest x1 30.4 us: on_device(): lax.all_to_all(mixed, 'tp', split_axis=0, concat_axis=1, tiled=True)]
    all_gather x3 -> x0, waiting for transfers between devices: 52.1 us -> none  [the longest x1 52 us: on_device(): lax.all_gather(exp_down, 'tp', axis=1, tiled=True)]
    add x75 -> x0, other arithmetic: 35.7 us -> none  [the longest x37 30 us: pair_join(): later_pair[0] * earlier[1] + later_pair[1]]
    all_gather x4 -> x0, blocking collectives: 32.5 us -> none  [carried_in(): gathered = jax.tree.map(lambda a: lax.all_gather(a, axis), part)]
    all_to_all x1 -> x0, blocking collectives: 29 us -> none  [on_device(): lax.all_to_all(outgoing.reshape(experts, capacity, width_model), 'sp', sp...]
    pad x72 -> x0, local copies, waits for them, and re-layouts: 22.4 us -> none  [the longest x36 14.7 us: on_device(): lax.associative_scan(pair_join, (jnp.flip(bwd_decay, 0), jnp.flip(bwd_dri...]
  transfers between devices with their start and end apart: 7 -> 0, of which waited for: 3 -> 0; matrix products, arithmetic and copies ran while one was open for 58% -> 0% of each run, Pallas kernels for 0% -> 0%
where the time goes in v1:
time: 277 us
  Pallas kernels  251 us (91%)
  matrix products  19.5 us (7%)
  other arithmetic  3.92 us (1%)
    pallas_call x1, Pallas kernels, on_device(): pl.pallas_call(functools.partial(mixer_kernel, dims), out_shape=(sds((row...  200 us
    pallas_call x1, Pallas kernels, on_device(): pl.pallas_call(functools.partial(return_kernel, dims), out_shape=sds((exp...  51.2 us
    dot_general x1, matrix products, on_device(): jnp.dot(hidden, down_full.reshape(T * F, D), preferred_element_type=f32)  10.1 us
    dot_general x1, matrix products, on_device(): gate_act = jnp.dot(flat, gate_full, preferred_element_type=f32)  6.63 us

profile of v1, /device:TPU:0, one launch (start us, length us, event | category | flops | bytes accessed | tf_op | source)
XLA Modules:
  0.0 276.9 jit_solution(2506260236939900451)
XLA Ops:
  0.0 0.0 copy-start
  0.0 0.7 constant_dynamic-slice_fusion.1
  0.7 0.1 copy.24
  0.8 0.1 eq.28
  1.0 0.2 fusion
  1.2 0.1 convert_element_type.31
  1.3 0.1 copy.25
  1.4 1.2 multiply_add_fusion
  2.6 1.3 compare_select_fusion.soft_ref
  3.9 200.3 %shard_map.163 = (bf16[128,2048]{1,0:T(8,128)(2,1)}, bf16[16,32,2048]{2,1,0:T(8,128)(2,1)}, bf16[2048,1024]{1,0:T(8,128)(2,1)}, bf16[2048,1024]{1,0:T(8,128)(2,1)}, bf16[1024,2048]{1,0:T(8,128)(2,1)}) custom-call(bf16[1024,256]{1,0:T(8,128)(2,1)} %mix_ref.1, bf16[1024,256]{1,0:T(8,128)(2,1)} %gate_ref.1, f32[4,256]{1,0:T(4,128)} %cw_ref.1, ...), custom_call_target="tpu_custom_call" | custom-call | tf_op jit(solution)/shard_map/pallas_call | solution.py:412
  204.2 0.0 copy-start.3
  204.2 6.6 %fusion.7 = f32[512,1024]{1,0:T(8,128)} fusion(bf16[512,2048]{1,0:T(8,128)(2,1)} %bitcast.18, bf16[2048,1024]{1,0:T(8,128)(2,1)} %get-tuple-element.12), kind=kOutput, calls=%fused_computation.22 | convolution fusion | flops 2147483648 | bytes 8388608 | tf_op jit(solution)/shard_map/dot_general | solution.py:452
  210.9 0.0 copy-done.3
  210.9 10.1 %convolution_convert_fusion = bf16[512,2048]{1,0:T(8,128)(2,1)} fusion(bf16[1024,2048]{1,0:T(8,128)(2,1)} %get-tuple-element.14, f32[512,1024]{1,0:T(8,128)} %fusion.7, bf16[512,2048]{1,0:T(8,128)(2,1)S(1)} %bitcast.19, bf16[2048,1024]{1,0:T(8,128)(2,1)} %get-tuple-element.13), kind=kOutput, calls=%fused_computation | convolution fusion | flops 4299161600 | bytes 14680064 | tf_op jit(solution)/shard_map/dot_general | solution.py:458
  220.9 0.0 copy-start.2
  220.9 51.2 %shard_map.164 = bf16[16,32,2048]{2,1,0:T(8,128)(2,1)} custom-call(bf16[16,32,2048]{2,1,0:T(8,128)(2,1)} %bitcast.14), custom_call_target="tpu_custom_call" | custom-call | tf_op jit(solution)/shard_map/pallas_call | solution.py:461
  272.1 0.0 copy-start.1
  272.1 0.0 copy-done
  272.1 0.0 copy-done.2
  272.1 0.1 select_reduce_fusion
  272.3 2.6 convolution_convert_fusion.1
  274.9 0.2 fusion.1
  275.1 0.8 slice.3
  275.9 0.0 copy-done.1
  275.9 1.1 fusion.4
  (3 shorter events, 0.0 us)
Async XLA Ops:
  0.0 272.1 %copy-start = (f32[1024,2]{0,1:T(2,128)S(1)}, f32[1024,2]{0,1:T(2,128)}, u32[]{:S(2)}) copy-start(f32[1024,2]{0,1:T(2,128)} %param.30) | copy-start | bytes 24580
  204.2 6.6 %copy-start.3 = (bf16[16,32,2048]{2,1,0:T(8,128)(2,1)S(1)}, bf16[16,32,2048]{2,1,0:T(8,128)(2,1)}, u32[]{:S(2)}) copy-start(bf16[16,32,2048]{2,1,0:T(8,128)(2,1)} %get-tuple-element.11) | copy-start | bytes 6291460
  220.9 51.2 %copy-start.2 = (s32[128,2]{0,1:T(2,128)S(1)}, s32[128,2]{0,1:T(2,128)}, u32[]{:S(2)}) copy-start(s32[128,2]{0,1:T(2,128)} %multiply_add_fusion) | copy-start | bytes 3076
  272.1 3.8 %copy-start.1 = (bf16[128,2048]{1,0:T(8,128)(2,1)S(1)}, bf16[128,2048]{1,0:T(8,128)(2,1)}, u32[]{:S(2)}) copy-start(bf16[128,2048]{1,0:T(8,128)(2,1)} %get-tuple-element.10) | copy-start | bytes 1572868

commit v2 on v1

--- a/solution.py
+++ b/solution.py
@@ -8,7 +8,6 @@
 from jax.sharding import PartitionSpec as P
 
 EPSILON = 1e-06
-HIGHEST_MODE = lax.Precision.HIGHEST
 MESH = pl.DeviceIdType.MESH
 HALO = 16
 SUB = 8
@@ -30,11 +29,6 @@
     )
     position = jnp.sum(jnp.where(matches, earlier_hits, 0.0), axis=1).astype(jnp.int32)
     return (flattened * capacity + position).reshape(row_count, top_count)
-
-
-def weight_table(slots, route_weights, total_slots):
-    matches = slots[..., None] == jnp.arange(total_slots, dtype=jnp.int32)
-    return jnp.sum(jnp.where(matches, route_weights[..., None], 0.0), axis=-2)
 
 
 def one_minus_exp(y):
@@ -66,22 +60,27 @@
     mix_ref, gate_ref, cw_ref, cb_ref, soft_ref, rg_ref, rb_ref, ig_ref, ib_ref,
     res_ref, gain_ref, slots_ref, op_hbm, eg_hbm, eu_hbm, ed_hbm,
     stream_ref, arrived_hbm, gf_hbm, uf_hbm, df_hbm,
-    xp, wh, wl, af, bf, ab, bb, mixed, tok, op, proj, outgoing, halo, summ, ends,
+    xp, wh, wl, af, bf, ab, bb, mixed, tok, op, proj, normed, outgoing, halo, summ, ends,
     bg, bu, bd,
     op_sem, own_sem, halo_send, halo_recv, sum_send, sum_recv,
-    mix_send, mix_recv, dis_send, dis_recv, z_send, z_recv, c_send, c_recv,
+    mix_send, mix_recv, row_send, row_recv, dis_send, dis_recv, z_send, z_recv, c_send, c_recv,
 ):
-    S, T, L, G = dims
+    S, T, L, G, H = dims
+    B = L // H
     seq, C = mix_ref.shape
     rows, D = res_ref.shape
-    slots = outgoing.shape[0]
-    cap = slots // (S * L)
+    held = outgoing.shape[1] // S
     heads, hd = rg_ref.shape[1], rg_ref.shape[2]
     F = eg_hbm.shape[2]
     sp = lax.axis_index("sp")
     tp = lax.axis_index("tp")
     q = tp // G
     g = lax.rem(tp, G)
+    half = q // B
+    kind = lax.rem(q, B)
+
+    def near_of(db, dg):
+        return (half * B + lax.rem(kind + db, B)) * G + lax.rem(g + dg, G)
 
     def place_of(dq, dg):
         return lax.rem(q + dq, L) * G + lax.rem(g + dg, G)
@@ -89,7 +88,7 @@
     op_copy = pltpu.make_async_copy(op_hbm, op, op_sem)
     op_copy.start()
     own_in = [
-        pltpu.make_async_copy(h.at[q], v, own_sem.at[i])
+        pltpu.make_async_copy(h.at[pl.ds(kind * H, H)], v, own_sem.at[i])
         for i, (h, v) in enumerate(((eg_hbm, bg), (eu_hbm, bu), (ed_hbm, bd)))
     ]
     for c in own_in:
@@ -100,7 +99,7 @@
     for ds in range(S):
         for dq in range(L):
             for dg in range(G):
-                if (ds or dq or dg) and (ds == 0 or dg == 0):
+                if (ds or dq or dg) and (ds == 0 or (dq == 0 and dg == 0)):
                     pl.semaphore_signal(
                         barrier, inc=1,
                         device_id=(lax.rem(sp + ds, S), place_of(dq, dg)),
@@ -123,44 +122,43 @@
     to_prev.start()
 
     def full_slot(ref, axis, place):
-        if len(ref.shape) == 3:
-            return ref.at[place]
+        if len(ref.shape) == 4:
+            return ref.at[:, place]
         start = pl.multiple_of(place * F, F)
-        return ref.at[:, pl.ds(start, F)] if axis else ref.at[pl.ds(start, F), :]
+        return ref.at[:, :, pl.ds(start, F)] if axis else ref.at[:, pl.ds(start, F), :]
 
     tensors = ((eg_hbm, gf_hbm, 1), (eu_hbm, uf_hbm, 1), (ed_hbm, df_hbm, 0))
-
-    def z_copies(dq):
+    column = kind * G + g
+
+    def z_copies(db):
+        to_kind = lax.rem(kind + db, B)
         return [
-            remote(src.at[lax.rem(q + dq, L)], full_slot(dst, axis, tp), z_send.at[dq, i],
-                   z_recv.at[dq, i], sp, place_of(dq, 0))
+            remote(src.at[pl.ds(to_kind * H, H)], full_slot(dst, axis, column), z_send.at[db, i],
+                   z_recv.at[db, i], sp, near_of(db, 0))
             for i, (src, dst, axis) in enumerate(tensors)
         ]
 
-    def core_copies(dq, i, own):
+    def core_copies(db, i, own):
         src, dst, axis = tensors[i]
-        origin = place_of(L - dq, 0)
-        at = full_slot(dst, axis, origin)
+        at = full_slot(dst, axis, lax.rem(kind + B - db, B) * G + g)
         return [
-            remote(own if own is not None else at, at, c_send.at[dq, dg, i], c_recv.at[dq, dg, i],
-                   sp, place_of(0, dg))
+            remote(own if own is not None else at, at, c_send.at[db, dg, i], c_recv.at[db, dg, i],
+                   sp, near_of(0, dg))
             for dg in range(1, G)
         ]
 
-    far = [dq for dq in range(1, L) if min(dq, L - dq) > 1]
-    near = [dq for dq in range(1, L) if min(dq, L - dq) == 1]
-    z_all = {dq: z_copies(dq) for dq in range(1, L)}
+    z_all = {db: z_copies(db) for db in range(1, B)}
     for i in range(3):
-        for dq in near:
-            z_all[dq][i].start()
+        for db in range(1, B):
+            z_all[db][i].start()
     own_out, core_all = [], {}
     for i, (src, dst, axis) in enumerate(tensors):
-        core_all[0, i] = core_copies(0, i, src.at[q])
+        core_all[0, i] = core_copies(0, i, src.at[pl.ds(kind * H, H)])
         for c in core_all[0, i]:
             c.start()
     for i, (buf, (src, dst, axis)) in enumerate(zip((bg, bu, bd), tensors)):
         own_in[i].wait()
-        c = pltpu.make_async_copy(buf, full_slot(dst, axis, tp), own_sem.at[3 + i])
+        c = pltpu.make_async_copy(buf, full_slot(dst, axis, column), own_sem.at[3 + i])
         c.start()
         own_out.append(c)
 
@@ -274,9 +272,6 @@
         c.start()
     own_move = pltpu.make_async_copy(block_rows(tp), tok.at[:, columns], own_sem.at[6])
     own_move.start()
-    for dq in far:
-        for c in z_all[dq]:
-            c.start()
     op_copy.wait()
     own_move.wait()
     for c in moves:
@@ -299,49 +294,62 @@
             res_ref[at, :].astype(jnp.float32) + norm_rows(proj[at, :], gain_ref[0:1, :])
         ).astype(jnp.bfloat16)
         stream_ref[at, :] = s
-        tok[at, :] = norm_rows(s, gain_ref[1:2, :]).astype(jnp.bfloat16)
+        normed[q, at, :] = norm_rows(s, gain_ref[1:2, :]).astype(jnp.bfloat16)
         return 0
 
     lax.fori_loop(0, rows // part, norms, 0)
-    slot_id = lax.broadcasted_iota(jnp.int32, (slots, rows), 0)
-    hit = slot_id == slots_ref[0:1, :]
-    for k in range(1, slots_ref.shape[0]):
-        hit = hit | (slot_id == slots_ref[k : k + 1, :])
-    selector = jnp.where(hit, 1.0, 0.0).astype(jnp.bfloat16)
-
-    def dispatch(n, _):
-        cols = pl.ds(pl.multiple_of(n * 256, 256), 256)
-        outgoing[:, cols] = (
-            jnp.dot(selector, tok[:, cols], preferred_element_type=jnp.float32)
-            .astype(jnp.bfloat16)
-        )
-        return 0
-
-    lax.fori_loop(0, D // 256, dispatch, 0)
+    shares = [
+        remote(normed.at[q], normed.at[q], row_send.at[dq], row_recv.at[dq], sp, place_of(dq, 0))
+        for dq in range(1, L)
+    ]
+    for c in shares:
+        c.start()
+    slot_id = lax.broadcasted_iota(jnp.int32, (S * held, rows), 0)
     sends = []
-    mine = sp * L + q
-    for ds in range(S):
-        for dq in range(L):
-            sp_to, q_to = lax.rem(sp + ds, S), lax.rem(q + dq, L)
-            src = outgoing.at[pl.ds(pl.multiple_of((sp_to * L + q_to) * cap, cap), cap), :]
-            if ds or dq:
-                k = ds * L + dq
-                sends.append(remote(src, arrived_hbm.at[mine], dis_send.at[k], dis_recv.at[k],
-                                    sp_to, q_to * G + g))
-            else:
-                sends.append(pltpu.make_async_copy(src, arrived_hbm.at[mine], own_sem.at[7]))
-    for c in sends:
-        c.start()
-    for dq in near + far:
+    for dq in range(L):
+        origin = lax.rem(q + L - dq, L)
+        if dq:
+            shares[dq - 1].wait_recv()
+        named = slots_ref[origin]
+        hit = slot_id == named[0:1]
+        for k in range(1, named.shape[0]):
+            hit = hit | (slot_id == named[k : k + 1])
+        selector = jnp.where(hit, 1.0, 0.0).astype(jnp.bfloat16)
+
+        def dispatch(n, _):
+            cols = pl.ds(pl.multiple_of(n * 256, 256), 256)
+            outgoing[dq, :, cols] = (
+                jnp.dot(selector, normed[origin, :, cols], preferred_element_type=jnp.float32)
+                .astype(jnp.bfloat16)
+            )
+            return 0
+
+        lax.fori_loop(0, D // 256, dispatch, 0)
+        cap = held // H
+        mine = sp * L + origin
+        for ds in range(S):
+            sp_to = lax.rem(sp + ds, S)
+            for j in range(H):
+                start = pl.multiple_of(sp_to * held + j * cap, cap)
+                src, dst = outgoing.at[dq, pl.ds(start, cap), :], arrived_hbm.at[j, mine]
+                if ds:
+                    c = remote(src, dst, dis_send.at[dq, ds, j], dis_recv.at[dq, ds, j], sp_to, tp)
+                else:
+                    c = pltpu.make_async_copy(src, dst, dis_send.at[dq, ds, j])
+                c.start()
+                sends.append(c)
+    for db in range(1, B):
         for i in range(3):
-            z_all[dq][i].wait_recv()
-            core_all[dq, i] = core_copies(dq, i, None)
-            for c in core_all[dq, i]:
+            z_all[db][i].wait_recv()
+            core_all[db, i] = core_copies(db, i, None)
+            for c in core_all[db, i]:
                 c.start()
     for c in sends:
         c.wait()
-    for dq in range(1, L):
-        for c in z_all[dq]:
+    for c in shares:
+        c.wait_send()
+    for db in range(1, B):
+        for c in z_all[db]:
             c.wait_send()
     for c in own_out:
         c.wait()
@@ -350,36 +358,90 @@
             c.wait()
 
 
-def return_kernel(dims, rows_hbm, back_hbm, own_sem, send, recv):
-    S, T, L, G = dims
+def return_kernel(
+    dims, rows_hbm, stream_ref, gain_ref, slots_ref, wt_ref, out_ref,
+    back, part_out, part_in, total, ret_send, ret_recv, mix_send, mix_recv,
+):
+    S, T, L, G, H = dims
     sp = lax.axis_index("sp")
     tp = lax.axis_index("tp")
     q = tp // G
     g = lax.rem(tp, G)
+    held = back.shape[1] // S
+    cap = held // H
+    rows, D = stream_ref.shape
     barrier = pltpu.get_barrier_semaphore()
-    peers = [
-        (ds, dq, lax.rem(sp + ds, S), lax.rem(q + dq, L))
-        for ds in range(S) for dq in range(L) if ds or dq
-    ]
-    for ds, dq, sp_to, q_to in peers:
-        pl.semaphore_signal(
-            barrier, inc=1, device_id=(sp_to, q_to * G + g), device_id_type=MESH
-        )
+    peers = [(lax.rem(sp + ds, S), tp) for ds in range(1, S)]
+    peers += [(sp, lax.rem(q + dq, L) * G + g) for dq in range(1, L)]
+    for peer in peers:
+        pl.semaphore_signal(barrier, inc=1, device_id=peer, device_id_type=MESH)
     pl.semaphore_wait(barrier, len(peers))
-    mine = sp * L + q
-    copies = [
-        pltpu.make_async_remote_copy(
-            src_ref=rows_hbm.at[sp_to * L + q_to], dst_ref=back_hbm.at[mine],
-            send_sem=send.at[ds * L + dq], recv_sem=recv.at[ds * L + dq],
-            device_id=(sp_to, q_to * G + g), device_id_type=MESH,
-        )
-        for ds, dq, sp_to, q_to in peers
-    ]
-    copies.append(pltpu.make_async_copy(rows_hbm.at[mine], back_hbm.at[mine], own_sem))
-    for c in copies:
-        c.start()
-    for c in copies:
+    order = list(range(1, L)) + [0]
+    copies = {dq: [] for dq in order}
+    for dq in order:
+        origin = lax.rem(q + dq, L)
+        for ds in range(S):
+            sp_to = lax.rem(sp + ds, S)
+            for j in range(H):
+                start = pl.multiple_of(sp * held + j * cap, cap)
+                src, dst = rows_hbm.at[j, sp_to * L + origin], back.at[dq, pl.ds(start, cap), :]
+                if ds:
+                    c = pltpu.make_async_remote_copy(
+                        src_ref=src, dst_ref=dst, send_sem=ret_send.at[dq, ds, j],
+                        recv_sem=ret_recv.at[dq, ds, j], device_id=(sp_to, tp),
+                        device_id_type=MESH,
+                    )
+                else:
+                    c = pltpu.make_async_copy(src, dst, ret_send.at[dq, ds, j])
+                c.start()
+                copies[dq].append(c)
+    slot_id = lax.broadcasted_iota(jnp.int32, (rows, S * held), 1)
+    shares = []
+    for dq in order:
+        origin = lax.rem(q + dq, L)
+        named, wts = slots_ref[origin], wt_ref[origin]
+        table = jnp.zeros((rows, S * held), jnp.float32)
+        for k in range(named.shape[1]):
+            table = jnp.where(slot_id == named[:, k : k + 1], wts[:, k : k + 1], table)
+        high, low = split_f32(table)
+        for c in copies[dq]:
+            c.wait()
+
+        def combine(n, _):
+            cols = pl.ds(pl.multiple_of(n * 256, 256), 256)
+            values = back[dq, :, cols]
+            mix = jnp.dot(high, values, preferred_element_type=jnp.float32)
+            mix = mix + jnp.dot(low, values, preferred_element_type=jnp.float32)
+            if dq:
+                part_out[dq, :, cols] = mix.astype(jnp.bfloat16)
+            else:
+                total[:, cols] = mix
+            return 0
+
+        lax.fori_loop(0, D // 256, combine, 0)
+        if dq:
+            c = pltpu.make_async_remote_copy(
+                src_ref=part_out.at[dq], dst_ref=part_in.at[dq], send_sem=mix_send.at[dq],
+                recv_sem=mix_recv.at[dq], device_id=(sp, origin * G + g), device_id_type=MESH,
+            )
+            c.start()
+            shares.append(c)
+    for c in shares:
         c.wait()
+    part = 32
+
+    def finish(n, _):
+        at = pl.ds(pl.multiple_of(n * part, part), part)
+        mix = total[at, :]
+        for dq in range(1, L):
+            mix = mix + part_in[dq, at, :].astype(jnp.float32)
+        mix = mix.astype(jnp.bfloat16)
+        out_ref[at, :] = (
+            stream_ref[at, :].astype(jnp.float32) + norm_rows(mix, gain_ref[2:3, :])
+        ).astype(jnp.bfloat16)
+        return 0
+
+    lax.fori_loop(0, rows // part, finish, 0)
 
 
 def on_device(
@@ -389,17 +451,27 @@
     S, T = lax.axis_size("sp"), lax.axis_size("tp")
     L, D, F = exp_gate.shape
     G = T // L
-    dims = (S, T, L, G)
+    H = 2 if L % 2 == 0 and L > 2 else 1
+    B = L // H
+    dims = (S, T, L, G, H)
     seq, C = mix_in.shape
     rows = residual.shape[0]
     top_count = routes.shape[1]
     experts = L * S
     cap = 2 * rows * top_count // experts
-    total_slots = experts * cap
-    own_start = lax.axis_index("tp") * rows
-    own_routes = lax.dynamic_slice_in_dim(routes, own_start, rows, 0)
-    own_weights = lax.dynamic_slice_in_dim(route_wt, own_start, rows, 0)
-    own_slots = slot_table(own_routes, experts, cap)
+    place = lax.axis_index("tp")
+    lane, kind = place % G, (place // G) % B
+
+    def same_lane(a):
+        blocks = a.reshape(L, G, rows, top_count)
+        return lax.dynamic_index_in_dim(blocks, lane, 1, False)
+
+    slots = jax.vmap(lambda block: slot_table(block, experts, cap))(same_lane(routes))
+    weights = same_lane(route_wt)
+    within = slots % (L * cap) - kind * (H * cap)
+    slots = jnp.where(
+        (within >= 0) & (within < H * cap), slots // (L * cap) * (H * cap) + within, -1
+    )
     soft = jax.nn.softplus(-decay_param)
     wide = F % 128 == 0
     vmem = pl.BlockSpec(memory_space=pltpu.VMEM)
@@ -407,12 +479,13 @@
     b16, f32 = jnp.bfloat16, jnp.float32
     dma = pltpu.SemaphoreType.DMA
     sds = jax.ShapeDtypeStruct
-    up_shape = (D, T * F) if wide else (T, D, F)
-    down_shape = (T * F, D) if wide else (T, F, D)
+    N = B * G
+    up_shape = (H, D, N * F) if wide else (H, N, D, F)
+    down_shape = (H, N * F, D) if wide else (H, N, F, D)
     stream, arrived, gate_full, up_full, down_full = pl.pallas_call(
         functools.partial(mixer_kernel, dims),
         out_shape=(
-            sds((rows, D), b16), sds((experts, cap, D), b16),
+            sds((rows, D), b16), sds((H, S * L, cap, D), b16),
             sds(up_shape, b16), sds(up_shape, b16), sds(down_shape, b16),
         ),
         in_specs=[vmem] * 12 + [hbm] * 4,
@@ -427,50 +500,51 @@
             pltpu.VMEM((rows, T * C), b16),
             pltpu.VMEM(out_proj.shape, b16),
             pltpu.VMEM((rows, D), b16),
-            pltpu.VMEM((total_slots, D), b16),
+            pltpu.VMEM((L, rows, D), b16),
+            pltpu.VMEM((L, S * H * cap, D), b16),
             pltpu.VMEM((2, HALO, C), b16),
             pltpu.VMEM((SUB, C), f32),
             pltpu.VMEM((S - 1, SUB, C), f32),
-            pltpu.VMEM((D, F), b16), pltpu.VMEM((D, F), b16), pltpu.VMEM((F, D), b16),
+            pltpu.VMEM((H, D, F), b16), pltpu.VMEM((H, D, F), b16), pltpu.VMEM((H, F, D), b16),
             dma, dma((8,)),
             dma((2,)), dma((2,)),
             dma((S - 1,)), dma((S - 1,)),
             dma((T,)), dma((T,)),
-            dma((experts,)), dma((experts,)),
-            dma((L, 3)), dma((L, 3)),
-            dma((L, G, 3)), dma((L, G, 3)),
+            dma((L,)), dma((L,)),
+            dma((L, S, H)), dma((L, S, H)),
+            dma((B, 3)), dma((B, 3)),
+            dma((B, G, 3)), dma((B, G, 3)),
         ],
         compiler_params=pltpu.CompilerParams(
             collective_id=0, has_side_effects=True, vmem_limit_bytes=56 * 1024 * 1024
         ),
     )(
         mix_in, gate_in, conv_w, conv_b.reshape(1, C), soft, recur_gate, recur_bias, input_gate,
-        input_bias, residual, norm_gain, own_slots.T, out_proj, exp_gate, exp_up, exp_down,
+        input_bias, residual, norm_gain, slots.transpose(0, 2, 1), out_proj, exp_gate, exp_up, exp_down,
     )
-    flat = arrived.reshape(total_slots, D)
-    if wide:
-        gate_act = jnp.dot(flat, gate_full, preferred_element_type=f32)
-        up_act = jnp.dot(flat, up_full, preferred_element_type=f32)
-    else:
-        gate_act = jnp.einsum("md,tdf->mtf", flat, gate_full, preferred_element_type=f32)
-        up_act = jnp.einsum("md,tdf->mtf", flat, up_full, preferred_element_type=f32)
-    hidden = (jax.nn.silu(gate_act) * up_act).astype(b16).reshape(total_slots, T * F)
-    out_rows = jnp.dot(
-        hidden, down_full.reshape(T * F, D), preferred_element_type=f32
+    flat = arrived.reshape(H, S * L * cap, D)
+    spec = "hmd,hdf->hmf" if wide else "hmd,hndf->hmnf"
+    gate_act = jnp.einsum(spec, flat, gate_full, preferred_element_type=f32)
+    up_act = jnp.einsum(spec, flat, up_full, preferred_element_type=f32)
+    hidden = (jax.nn.silu(gate_act) * up_act).astype(b16).reshape(H, S * L * cap, N * F)
+    out_rows = jnp.einsum(
+        "hmf,hfd->hmd", hidden, down_full.reshape(H, N * F, D), preferred_element_type=f32
     ).astype(b16)
-    returned = pl.pallas_call(
+    return pl.pallas_call(
         functools.partial(return_kernel, dims),
-        out_shape=sds((experts, cap, D), b16),
-        in_specs=[hbm],
-        out_specs=hbm,
-        scratch_shapes=[dma, dma((experts,)), dma((experts,))],
+        out_shape=sds((rows, D), b16),
+        in_specs=[hbm] + [vmem] * 4,
+        out_specs=vmem,
+        scratch_shapes=[
+            pltpu.VMEM((L, S * H * cap, D), b16),
+            pltpu.VMEM((L, rows, D), b16),
+            pltpu.VMEM((L, rows, D), b16),
+            pltpu.VMEM((rows, D), f32),
+            dma((L, S, H)), dma((L, S, H)),
+            dma((L,)), dma((L,)),
+        ],
         compiler_params=pltpu.CompilerParams(collective_id=1, has_side_effects=True),
-    )(out_rows.reshape(experts, cap, D))
-    values = returned.reshape(total_slots, D).astype(f32)
-    own_table = weight_table(own_slots, own_weights, total_slots)
-    mixture = jnp.dot(own_table, values, precision=HIGHEST_MODE).astype(b16)
-    mixture = lax.optimization_barrier(mixture)
-    return (stream.astype(f32) + norm_rows(mixture, norm_gain[2])).astype(b16)
+    )(out_rows.reshape(H, S * L, cap, D), stream, norm_gain, slots, weights)
 
 
 def solution(mesh):

time: 277 us -> 253 us (0.913)
  Pallas kernels: 251 us -> 227 us
  local copies, waits for them, and re-layouts: 1.94 us -> 5.77 us
    pallas_call x1, Pallas kernels: 200 us -> 152 us  [on_device(): pl.pallas_call(functools.partial(mixer_kernel, dims), out_shape=(sds((row...]
    pallas_call x1, Pallas kernels: 51.2 us -> 74.8 us  [on_device(): pl.pallas_call(functools.partial(return_kernel, dims), out_shape=sds((row...]
    unnamed x8 -> x7, local copies, waits for them, and re-layouts: 0.02 us -> 2.91 us
    dot_general x4 -> x2, matrix products: 19.5 us -> 17.1 us  [the longest x1 11.3 us: on_device(): jnp.einsum('hmf,hfd->hmd', hidden, down_full.reshape(H, N * F, D), prefer...]
where the time goes in v2:
time: 253 us; the launch traced here: 252 us
  Pallas kernels  227 us (90%)
  matrix products  17.3 us (7%)
  local copies, waits for them, and re-layouts  5.77 us (2%)
    pallas_call x1, Pallas kernels, on_device(): pl.pallas_call(functools.partial(mixer_kernel, dims), out_shape=(sds((row...  152 us
    pallas_call x1, Pallas kernels, on_device(): pl.pallas_call(functools.partial(return_kernel, dims), out_shape=sds((row...  74.8 us
    dot_general x1, matrix products, on_device(): jnp.einsum('hmf,hfd->hmd', hidden, down_full.reshape(H, N * F, D), prefer...  11.3 us
    dot_general x1, matrix products, on_device(): gate_act = jnp.einsum(spec, flat, gate_full, preferred_element_type=f32)  5.79 us

profile of v2, /device:TPU:0, one launch (start us, length us, event | category | flops | bytes accessed | tf_op | source)
XLA Modules:
  0.0 251.6 jit_solution(12365589115195929251)
XLA Ops:
  0.0 0.7 reshape.27
  0.7 0.2 copy.27
  0.9 0.1 copy.28
  1.0 0.2 select_reduce_fusion
  1.2 0.1 copy.29
  1.4 1.0 copy.30
  2.4 0.2 copy.33
  2.6 0.3 fusion.4.slots_ref
  2.9 0.0 copy-start
  2.9 0.7 copy.31.slots_ref
  3.6 1.3 compare_select_fusion.soft_ref
  4.9 152.0 %shard_map.163 = (bf16[128,2048]{1,0:T(8,128)(2,1)}, bf16[2,16,32,2048]{3,2,1,0:T(8,128)(2,1)}, bf16[2,2048,512]{2,1,0:T(8,128)(2,1)}, bf16[2,2048,512]{2,1,0:T(8,128)(2,1)}, bf16[2,512,2048]{2,1,0:T(8,128)(2,1)}) custom-call(bf16[1024,256]{1,0:T(8,128)(2,1)} %mix_ref.1, bf16[1024,256]{1,0:T(8,128)(2,1)} %gate_ref.1, f32[4,256]{1,0:T(4,128)} %cw_ref.1, ...), custom_call_target="tpu_custom_call" | custom-call | tf_op jit(solution)/shard_map/pallas_call | solution.py:485
  156.9 0.0 copy-done
  156.9 5.8 %fusion.9 = f32[2,512,512]{2,1,0:T(8,128)S(1)} fusion(bf16[2,512,2048]{2,1,0:T(8,128)(2,1)} %bitcast.35, bf16[2,2048,512]{2,1,0:T(8,128)(2,1)} %get-tuple-element.11), kind=kOutput, calls=%fused_computation.24 | convolution fusion | flops 2147483648 | bytes 10485760 | tf_op jit(solution)/shard_map/hmd,hdf->hmf/dot_general | solution.py:527
  162.7 0.0 copy-start.1
  162.7 11.3 %convolution_convert_fusion = bf16[2,512,2048]{2,1,0:T(8,128)(2,1)} fusion(bf16[2,512,2048]{2,1,0:T(8,128)(2,1)} %get-tuple-element.13, f32[2,512,512]{2,1,0:T(8,128)S(1)} %fusion.9, bf16[2,512,2048]{2,1,0:T(8,128)(2,1)} %bitcast.36, bf16[2,2048,512]{2,1,0:T(8,128)(2,1)} %get-tuple-element.12), kind=kOutput, calls=%fused_computation | convolution fusion | flops 4300210176 | bytes 18874368 | tf_op jit(solution)/shard_map/hmf,hfd->hmd/dot_general | solution.py:530
  174.0 0.0 copy-done.1
  174.0 0.9 copy.34
  174.9 74.8 %shard_map.164 = bf16[128,2048]{1,0:T(8,128)(2,1)} custom-call(bf16[2,16,32,2048]{3,2,1,0:T(8,128)(2,1)} %bitcast.28, bf16[128,2048]{1,0:T(8,128)(2,1)} %get-tuple-element.14.stream_ref, f32[3,2048]{1,0:T(4,128)} %gain_ref.3, s32[4,128,2]{2,1,0:T(8,128)} %copy-done, f32[4,128,2]{2,1,0:T(8,128)} %bitcast.30), custom_call_target="tpu_custom_call" | custom-call | tf_op jit(solution)/shard_map/pallas_call | solution.py:533
  249.7 1.9 copy.37
  (5 shorter events, 0.1 us)
Async XLA Ops:
  2.9 154.0 %copy-start = (s32[4,128,2]{2,1,0:T(8,128)}, s32[4,128,2]{2,1,0:T(8,128)S(1)}, u32[]{:S(2)}) copy-start(s32[4,128,2]{2,1,0:T(8,128)S(1)} %fusion.4.slots_ref) | copy-start | bytes 12292
  162.7 11.3 %copy-start.1 = (f32[1024,2]{0,1:T(2,128)S(1)}, f32[1024,2]{0,1:T(2,128)}, u32[]{:S(2)}) copy-start(f32[1024,2]{0,1:T(2,128)} %param.30) | copy-start | bytes 24580

commit v3 on v2

--- a/solution.py
+++ b/solution.py
@@ -148,9 +148,8 @@
         ]
 
     z_all = {db: z_copies(db) for db in range(1, B)}
-    for i in range(3):
-        for db in range(1, B):
-            z_all[db][i].start()
+    for db in range(1, B):
+        z_all[db][0].start()
     own_out, core_all = [], {}
     for i, (src, dst, axis) in enumerate(tensors):
         core_all[0, i] = core_copies(0, i, src.at[pl.ds(kind * H, H)])
@@ -272,6 +271,8 @@
         c.start()
     own_move = pltpu.make_async_copy(block_rows(tp), tok.at[:, columns], own_sem.at[6])
     own_move.start()
+    for db in range(1, B):
+        z_all[db][1].start()
     op_copy.wait()
     own_move.wait()
     for c in moves:
@@ -304,6 +305,8 @@
     ]
     for c in shares:
         c.start()
+    for db in range(1, B):
+        z_all[db][2].start()
     slot_id = lax.broadcasted_iota(jnp.int32, (S * held, rows), 0)
     sends = []
     for dq in range(L):

time: 253 us -> 216 us (0.85)
  Pallas kernels: 227 us -> 190 us
    pallas_call x1, Pallas kernels: 152 us -> 123 us  [on_device(): pl.pallas_call(functools.partial(mixer_kernel, dims), out_shape=(sds((row...]
    pallas_call x1, Pallas kernels: 74.8 us -> 67.7 us  [on_device(): pl.pallas_call(functools.partial(return_kernel, dims), out_shape=sds((row...]
where the time goes in v3:
time: 216 us; the launch traced here: 215 us
  Pallas kernels  190 us (88%)
  matrix products  17.3 us (8%)
  local copies, waits for them, and re-layouts  5.77 us (3%)
    pallas_call x1, Pallas kernels, on_device(): pl.pallas_call(functools.partial(mixer_kernel, dims), out_shape=(sds((row...  123 us
    pallas_call x1, Pallas kernels, on_device(): pl.pallas_call(functools.partial(return_kernel, dims), out_shape=sds((row...  67.7 us
    dot_general x1, matrix products, on_device(): jnp.einsum('hmf,hfd->hmd', hidden, down_full.reshape(H, N * F, D), prefer...  11.3 us
    dot_general x1, matrix products, on_device(): gate_act = jnp.einsum(spec, flat, gate_full, preferred_element_type=f32)  5.79 us

profile of v3, /device:TPU:0, one launch (start us, length us, event | category | flops | bytes accessed | tf_op | source)
XLA Modules:
  0.0 215.3 jit_solution(12028235832322707256)
XLA Ops:
  0.0 0.7 reshape.27
  0.7 0.2 copy.27
  0.9 0.1 copy.28
  1.0 0.2 select_reduce_fusion
  1.2 0.1 copy.29
  1.4 1.0 copy.30
  2.4 0.2 copy.33
  2.6 0.3 fusion.4.slots_ref
  2.9 0.0 copy-start
  2.9 0.7 copy.31.slots_ref
  3.6 1.3 compare_select_fusion.soft_ref
  4.9 122.7 %shard_map.163 = (bf16[128,2048]{1,0:T(8,128)(2,1)}, bf16[2,16,32,2048]{3,2,1,0:T(8,128)(2,1)}, bf16[2,2048,512]{2,1,0:T(8,128)(2,1)}, bf16[2,2048,512]{2,1,0:T(8,128)(2,1)}, bf16[2,512,2048]{2,1,0:T(8,128)(2,1)}) custom-call(bf16[1024,256]{1,0:T(8,128)(2,1)} %mix_ref.1, bf16[1024,256]{1,0:T(8,128)(2,1)} %gate_ref.1, f32[4,256]{1,0:T(4,128)} %cw_ref.1, ...), custom_call_target="tpu_custom_call" | custom-call | tf_op jit(solution)/shard_map/pallas_call | solution.py:488
  127.7 0.0 copy-done
  127.7 5.8 %fusion.9 = f32[2,512,512]{2,1,0:T(8,128)S(1)} fusion(bf16[2,512,2048]{2,1,0:T(8,128)(2,1)} %bitcast.35, bf16[2,2048,512]{2,1,0:T(8,128)(2,1)} %get-tuple-element.11), kind=kOutput, calls=%fused_computation.24 | convolution fusion | flops 2147483648 | bytes 10485760 | tf_op jit(solution)/shard_map/hmd,hdf->hmf/dot_general | solution.py:530
  133.5 0.0 copy-start.1
  133.5 11.3 %convolution_convert_fusion = bf16[2,512,2048]{2,1,0:T(8,128)(2,1)} fusion(bf16[2,512,2048]{2,1,0:T(8,128)(2,1)} %get-tuple-element.13, f32[2,512,512]{2,1,0:T(8,128)S(1)} %fusion.9, bf16[2,512,2048]{2,1,0:T(8,128)(2,1)} %bitcast.36, bf16[2,2048,512]{2,1,0:T(8,128)(2,1)} %get-tuple-element.12), kind=kOutput, calls=%fused_computation | convolution fusion | flops 4300210176 | bytes 18874368 | tf_op jit(solution)/shard_map/hmf,hfd->hmd/dot_general | solution.py:533
  144.8 0.0 copy-done.1
  144.8 0.9 copy.34
  145.7 67.7 %shard_map.164 = bf16[128,2048]{1,0:T(8,128)(2,1)} custom-call(bf16[2,16,32,2048]{3,2,1,0:T(8,128)(2,1)} %bitcast.28, bf16[128,2048]{1,0:T(8,128)(2,1)} %get-tuple-element.14.stream_ref, f32[3,2048]{1,0:T(4,128)} %gain_ref.3, s32[4,128,2]{2,1,0:T(8,128)} %copy-done, f32[4,128,2]{2,1,0:T(8,128)} %bitcast.30), custom_call_target="tpu_custom_call" | custom-call | tf_op jit(solution)/shard_map/pallas_call | solution.py:536
  213.4 1.9 copy.37
  (5 shorter events, 0.1 us)
Async XLA Ops:
  2.9 124.8 %copy-start = (s32[4,128,2]{2,1,0:T(8,128)}, s32[4,128,2]{2,1,0:T(8,128)S(1)}, u32[]{:S(2)}) copy-start(s32[4,128,2]{2,1,0:T(8,128)S(1)} %fusion.4.slots_ref) | copy-start | bytes 12292
  133.5 11.3 %copy-start.1 = (f32[1024,2]{0,1:T(2,128)S(1)}, f32[1024,2]{0,1:T(2,128)}, u32[]{:S(2)}) copy-start(f32[1024,2]{0,1:T(2,128)} %param.30) | copy-start | bytes 24580
